TPU v7x, 32 devices: a whole 2x2x4 slice. The times are simulated.
32 devices in a mesh: sp: 4 (over z), fs: 4 (over y, x), tp: 2 (over core).
Axes of the slice: x: 2, y: 2, z: 4, core: 2. Of those that a mesh axis runs over, the one named last changes fastest.
Arguments:
- tokens: bfloat16 [4, 1024, 2048], P('fs', ('sp', 'tp')), may hold values from -6 to 6
- norm_gain: float32 [2048], replicated, may hold values from 0.1 to 1.9
- w_conv_gate: bfloat16 [2048, 1024], P('sp', 'tp'), may hold values from -0.125 to 0.125
- w_conv_in: bfloat16 [2048, 1024], P('sp', 'tp'), may hold values from -0.125 to 0.125
- w_conv_value: bfloat16 [2048, 1024], P('sp', 'tp'), may hold values from -0.125 to 0.125
- conv_taps: float32 [3, 1024], P(None, 'tp'), may hold values from -3.5 to 3.5
- w_receptance: bfloat16 [2048, 1024], P('sp', 'tp'), may hold values from -0.125 to 0.125
- w_key: bfloat16 [2048, 1024], P('sp', 'tp'), may hold values from -0.125 to 0.125
- w_value: bfloat16 [2048, 1024], P('sp', 'tp'), may hold values from -0.125 to 0.125
- w_decay_down: bfloat16 [2048, 128], P('sp'), may hold values from -0.125 to 0.125
- w_decay_up: bfloat16 [128, 1024], P(None, 'tp'), may hold values from -0.75 to 0.75
- decay_base: float32 [1024], P('tp'), may hold values from -12.5 to -3
- decay_shift: float32 [4, 1024, 1024], P('fs', 'sp', 'tp'), may hold values from -2.1 to 0
- w_rate_down: bfloat16 [2048, 128], P('sp'), may hold values from -0.125 to 0.125
- w_rate_up: bfloat16 [128, 1024], P(None, 'tp'), may hold values from -0.5 to 0.5
- rate_base: float32 [1024], P('tp'), may hold values from -10 to 1
- key_scale: float32 [1024], P('tp'), may hold values from 0.25 to 2.5
- key_mix: float32 [1024], P('tp'), may hold values from 0.1 to 0.7
- group_gain: float32 [1024], P('tp'), may hold values from 0.1 to 1.9
- w_out_conv: bfloat16 [1024, 2048], P('tp', 'sp'), may hold values from -0.125 to 0.125
- w_out_state: bfloat16 [1024, 2048], P('tp', 'sp'), may hold values from -0.125 to 0.125
Outputs:
- mixed: bfloat16 [4, 1024, 2048], P('fs', ('sp', 'tp'))
All inputs are finite; a program needn't handle non-finite values.
Results may differ from a plain program's by a relative error of at most 0.015.
Values may be sent and summed in bfloat16 or wider, within the bound.
A program may use at most 128 MiB of HBM per device.

v0:
```python
import functools

import jax
import jax.numpy as jnp
from jax import lax
from jax.experimental import pallas as pl
from jax.experimental.pallas import tpu as pltpu
from jax.sharding import PartitionSpec as P

HEAD = 64
CHUNK = 64
norm_eps = 1e-06
group_eps = 0.00064
f32, bf16 = jnp.float32, jnp.bfloat16

NN = (((1,), (0,)), ((), ()))
NT = (((1,), (1,)), ((), ()))
TN = (((0,), (0,)), ((), ()))


def dot1(a, b, dims):
    return lax.dot_general(a.astype(bf16), b.astype(bf16), dims, preferred_element_type=f32)


def dot3(a, b, dims):
    ah, bh = a.astype(bf16), b.astype(bf16)
    al, bl = (a - ah.astype(f32)).astype(bf16), (b - bh.astype(f32)).astype(bf16)
    d = functools.partial(lax.dot_general, dimension_numbers=dims, preferred_element_type=f32)
    return d(ah, bh) + (d(ah, bl) + d(al, bh))


def stack_heads(x, lanes_low):
    return jnp.concatenate([jnp.where(lanes_low, x, 0.0), jnp.where(lanes_low, 0.0, x)], axis=0)


def fold(x):
    half = x.shape[0] // 2
    return x[:half] + x[half:]


def state_kernel(
    recv_ref, key_ref, val_ref, dlow_ref, rlow_ref, wdu_ref, wru_ref, shift_ref, par_ref,
    q_ref, l_ref, ma_ref,
):
    tokens, width = recv_ref.shape
    par = par_ref[...]
    decay_base, rate_base, key_scale, key_mix = (par[i : i + 1] for i in range(4))
    act = jnp.tanh(dlow_ref[...].astype(f32)).astype(bf16)
    pre = decay_base + lax.dot_general(act, wdu_ref[...], NN, preferred_element_type=f32)
    log_decay = shift_ref[0] - jnp.exp(-0.5) * jax.nn.sigmoid(pre)
    rate = jax.nn.sigmoid(
        rate_base + lax.dot_general(rlow_ref[...], wru_ref[...], NN, preferred_element_type=f32)
    )
    key = key_ref[...].astype(f32)
    scaled = key * key_scale
    lane_low = lax.broadcasted_iota(jnp.int32, (1, width), 1) < HEAD
    sq = scaled * scaled
    low_sum = jnp.sum(jnp.where(lane_low, sq, 0.0), axis=-1, keepdims=True)
    high_sum = jnp.sum(jnp.where(lane_low, 0.0, sq), axis=-1, keepdims=True)
    erase = scaled * lax.rsqrt(jnp.where(lane_low, low_sum, high_sum) + norm_eps)
    write = key * (1.0 + (rate - 1.0) * key_mix)
    replace = erase * rate
    recv = recv_ref[...].astype(f32)
    val = val_ref[...].astype(f32)

    rows = 2 * CHUNK
    ri = lax.broadcasted_iota(jnp.int32, (rows, rows), 0)
    ci = lax.broadcasted_iota(jnp.int32, (rows, rows), 1)
    same = (ri < CHUNK) == (ci < CHUNK)
    strict = jnp.logical_and(same, ri > ci)
    causal = jnp.logical_and(same, ri >= ci)
    eye = (ri == ci).astype(f32)
    tri = jnp.where(
        lax.broadcasted_iota(jnp.int32, (CHUNK, CHUNK), 0)
        >= lax.broadcasted_iota(jnp.int32, (CHUNK, CHUNK), 1),
        1.0,
        0.0,
    ).astype(f32)
    wi = lax.broadcasted_iota(jnp.int32, (width, width), 0)
    wj = lax.broadcasted_iota(jnp.int32, (width, width), 1)
    weye = wi == wj

    parts = []
    for c in range(tokens // CHUNK):
        sl = slice(c * CHUNK, (c + 1) * CHUNK)
        ld = log_decay[sl]
        incl = lax.dot_general(tri, ld, NN, precision=lax.Precision.HIGHEST, preferred_element_type=f32)
        final = incl[CHUNK - 1 : CHUNK]
        mid = incl[CHUNK // 2 - 1 : CHUNK // 2]
        excl = incl - ld
        up, back = jnp.exp(incl - mid), jnp.exp(mid - incl)
        st = lambda x: stack_heads(x, lane_low)
        e_mid = st(-erase[sl] * jnp.exp(excl - mid))
        q_mid = st(recv[sl] * up)
        r_back = st(replace[sl] * back)
        k_back = st(write[sl] * back)
        v = st(val[sl])
        e_now = st(-erase[sl] * jnp.exp(excl))
        q_now = st(recv[sl] * jnp.exp(incl))
        tail = jnp.exp(final - incl)
        r_end = st(replace[sl] * tail)
        k_end = st(write[sl] * tail)
        pairs = dot1(
            jnp.concatenate([e_mid, q_mid], axis=0), jnp.concatenate([r_back, k_back], axis=0), NT
        )
        x = jnp.where(strict, pairs[:rows, :rows], 0.0)
        ek = jnp.where(strict, pairs[:rows, rows:], 0.0)
        qr = jnp.where(causal, pairs[rows:, :rows], 0.0)
        qk = jnp.where(causal, pairs[rows:, rows:], 0.0)
        ekv_qkv = dot1(jnp.concatenate([ek, qk], axis=0), v, NN)
        inv = eye + x
        power = dot1(x, x, NN)
        reached = 2
        while reached < CHUNK:
            if reached * 2 < CHUNK:
                step = dot1(jnp.concatenate([inv, power], axis=0), power, NN)
                inv, power = inv + step[:rows], step[rows:]
            else:
                inv = inv + dot1(inv, power, NN)
            reached *= 2
        solved = dot1(inv, jnp.concatenate([e_now, ekv_qkv[:rows]], axis=1), NN)
        start_map, local_erase = solved[:, :width], solved[:, width:]
        seen = dot1(qr, solved, NN)
        query_map = fold(q_now + seen[:, :width])
        local_out = fold(seen[:, width:] + ekv_qkv[rows:])
        decay_diag = jnp.where(weye, jnp.exp(final), 0.0)
        step_map = decay_diag + dot3(start_map, r_end, TN)
        carried = dot1(local_erase, r_end, TN) + dot1(v, k_end, TN)
        parts.append((query_map, local_out, step_map, carried))

    total_map = total_add = None
    for c, (query_map, local_out, step_map, carried) in enumerate(parts):
        sl = slice(c * CHUNK, (c + 1) * CHUNK)
        if c == 0:
            q_ref[sl] = query_map.astype(bf16)
            l_ref[sl] = local_out
            total_map, total_add = step_map, carried
        else:
            q_ref[sl] = dot1(query_map, total_map, NT).astype(bf16)
            l_ref[sl] = local_out + dot1(query_map, total_add, NT)
            total_map, total_add = (
                dot3(total_map, step_map, NN),
                dot3(total_add, step_map, NN) + carried,
            )
    ma_ref[0, 0] = fold(total_map).astype(bf16)
    ma_ref[0, 1] = fold(total_add).astype(bf16)


def finish_kernel(n_sp, place_ref, q_ref, l_ref, ma_ref, gain_ref, out_ref):
    width = q_ref.shape[1]
    place = place_ref[0]
    wi = lax.broadcasted_iota(jnp.int32, (width, width), 0)
    wj = lax.broadcasted_iota(jnp.int32, (width, width), 1)
    same = (wi < HEAD) == (wj < HEAD)
    widen = lambda x: jnp.where(same, jnp.concatenate([x, x], axis=0), 0.0)
    state = jnp.zeros((width, width), f32)
    for hop in range(n_sp - 1):
        new = dot3(state, widen(ma_ref[hop, 0, 0].astype(f32)), NN) + widen(
            ma_ref[hop, 0, 1].astype(f32)
        )
        state = jnp.where(hop < place, new, state)
    out = l_ref[...] + dot1(q_ref[...], state, NT)
    low = lax.broadcasted_iota(jnp.int32, (1, width), 1) < HEAD

    def head_mean(x):
        a = jnp.sum(jnp.where(low, x, 0.0), axis=-1, keepdims=True)
        b = jnp.sum(jnp.where(low, 0.0, x), axis=-1, keepdims=True)
        return jnp.where(low, a, b) * (1.0 / HEAD)

    centered = out - head_mean(out)
    var = head_mean(centered * centered)
    out_ref[...] = (centered * lax.rsqrt(var + group_eps) * gain_ref[...]).astype(bf16)


MESH = pl.DeviceIdType.MESH


def greet(peers):
    barrier = pltpu.get_barrier_semaphore()
    for peer in peers:
        pl.semaphore_signal(barrier, inc=1, device_id=peer, device_id_type=MESH)
    return barrier


def send(src, dst, send_sem, recv_sem, peer):
    return pltpu.make_async_remote_copy(
        src_ref=src, dst_ref=dst, send_sem=send_sem, recv_sem=recv_sem,
        device_id=peer, device_id_type=MESH,
    )


def gather_kernel(
    n_sp, n_fs, tok_ref, shift_ref, *refs
):
    w_refs, refs = refs[:5], refs[5:]
    (
        toks, weights, shifts, w_sem, local_sem, tok_send, tok_recv, pair_send, pair_recv,
        right_send, left_send, w_recv, shift_send, shift_recv,
    ) = refs
    width = shifts.shape[-1]
    sp, fs, tp = lax.axis_index("sp"), lax.axis_index("fs"), lax.axis_index("tp")
    partner = {"tp": 1 - tp}
    others = [lax.rem(fs + d, n_fs) for d in range(1, n_fs)]
    start_lane, pieces = 0, []
    for k, ref in enumerate(w_refs):
        wide = width if k < 3 else ref.shape[1]
        source = ref.at[:, pl.ds(pl.multiple_of(fs * width, width), width)] if k < 3 else ref
        pieces.append(
            pltpu.make_async_copy(
                source, weights.at[sp, :, pl.ds(start_lane, wide)], w_sem.at[k]
            )
        )
        start_lane += wide
    for piece in pieces:
        piece.start()

    def shift_block(f):
        return shift_ref.at[:, pl.ds(pl.multiple_of(f * width, width), width)]

    barrier = greet([partner] + [{"fs": f} for f in others])
    has_left, has_right = sp > 0, sp < n_sp - 1

    @pl.when(has_left)
    def _():
        pl.semaphore_signal(barrier, inc=1, device_id={"sp": sp - 1}, device_id_type=MESH)

    @pl.when(has_right)
    def _():
        pl.semaphore_signal(barrier, inc=1, device_id={"sp": sp + 1}, device_id_type=MESH)

    pl.semaphore_wait(barrier, n_fs + has_left.astype(jnp.int32) + has_right.astype(jnp.int32))

    def rightward(j):
        src = weights.at[j]
        return send(src, weights.at[j], right_send.at[j], w_recv.at[j], {"sp": sp + 1})

    def leftward(j):
        src = weights.at[j]
        return send(src, weights.at[j], left_send.at[j], w_recv.at[j], {"sp": sp - 1})

    own_right, own_left = rightward(sp), leftward(sp)
    for piece in pieces:
        piece.wait()

    @pl.when(has_right)
    def _():
        own_right.start()

    @pl.when(has_left)
    def _():
        own_left.start()

    own_s = pltpu.make_async_copy(shift_block(fs), shifts.at[fs], local_sem.at[0])
    own_t = pltpu.make_async_copy(tok_ref, toks.at[fs, tp], local_sem.at[1])
    own_s.start()
    own_t.start()
    token_sends = [
        send(tok_ref, toks.at[fs, tp], tok_send.at[f], tok_recv.at[fs], {"fs": f}) for f in others
    ]
    for copy in token_sends:
        copy.start()
    pair_own = send(tok_ref, toks.at[fs, tp], pair_send.at[fs], pair_recv.at[fs], partner)
    pair_own.start()
    shift_sends = [
        send(shift_block(f), shifts.at[fs], shift_send.at[f], shift_recv.at[fs], {"fs": f})
        for f in others
    ]
    for copy in shift_sends:
        copy.start()

    def from_peer(f):
        return send(toks.at[f, tp], toks.at[f, tp], tok_send.at[f], tok_recv.at[f], {"fs": f})

    def to_partner(f):
        return send(toks.at[f, tp], toks.at[f, tp], pair_send.at[f], pair_recv.at[f], partner)

    def from_partner(f):
        there = toks.at[f, 1 - tp]
        return send(there, there, pair_send.at[f], pair_recv.at[f], partner)

    for k in range(1, n_sp):

        @pl.when(sp >= k)
        def _():
            rightward(sp - k).wait_recv()

            @pl.when(has_right)
            def _():
                rightward(sp - k).start()

        @pl.when(sp + k < n_sp)
        def _():
            leftward(sp + k).wait_recv()

            @pl.when(has_left)
            def _():
                leftward(sp + k).start()

        if k == 1:
            for f in reversed(others):
                from_peer(f).wait_recv()
                to_partner(f).start()

    own_s.wait()
    own_t.wait()
    for copy in token_sends + shift_sends:
        copy.wait_send()
    for f in others:
        send(shifts.at[f], shifts.at[f], shift_send.at[f], shift_recv.at[f], {"fs": f}).wait_recv()
    pair_own.wait_send()
    for f in others:
        to_partner(f).wait_send()
    for f in [fs] + others:
        from_partner(f).wait_recv()

    @pl.when(has_right)
    def _():
        own_right.wait_send()

    @pl.when(has_left)
    def _():
        own_left.wait_send()

    for k in range(1, n_sp):

        @pl.when(jnp.logical_and(sp >= k, has_right))
        def _():
            rightward(sp - k).wait_send()

        @pl.when(jnp.logical_and(sp + k < n_sp, has_left))
        def _():
            leftward(sp + k).wait_send()


def reduce_kernel(
    n_fs, part_ref, out_ref, from_pair, sums, from_fs, pair_send, pair_recv, fs_send, fs_recv
):
    fs, tp = lax.axis_index("fs"), lax.axis_index("tp")
    partner = {"tp": 1 - tp}
    order = [lax.rem(fs + d, n_fs) for d in range(1, n_fs)] + [fs]
    barrier = greet([partner] + [{"fs": f} for f in order[:-1]])
    pl.semaphore_wait(barrier, n_fs)
    swaps = [
        send(part_ref.at[f, 1 - tp], from_pair.at[d], pair_send.at[d], pair_recv.at[d], partner)
        for d, f in enumerate(order)
    ]
    for copy in swaps:
        copy.start()
    sends = []
    for d, f in enumerate(order):
        swaps[d].wait_recv()
        total = part_ref[f, tp].astype(f32) + from_pair[d].astype(f32)
        sums[d] = total.astype(bf16)
        if d < n_fs - 1:
            copy = send(sums.at[d], from_fs.at[d], fs_send.at[d], fs_recv.at[d], {"fs": f})
            copy.start()
            sends.append(copy)
    for copy in sends:
        copy.wait_recv()
    result = sums[n_fs - 1].astype(f32)
    for d in range(n_fs - 1):
        result = result + from_fs[d].astype(f32)
    out_ref[...] = result.astype(bf16)
    for copy in sends:
        copy.wait_send()
    for copy in swaps:
        copy.wait_send()


def gather_inputs(n_sp, n_fs, n_tp, tok, shift, weights):
    dma = lambda n: pltpu.SemaphoreType.DMA((n,))
    depth, width = weights[0].shape[0], weights[0].shape[1] // n_fs
    columns = 3 * width + weights[3].shape[1] + weights[4].shape[1]
    vmem = pl.BlockSpec(memory_space=pltpu.VMEM)
    return pl.pallas_call(
        functools.partial(gather_kernel, n_sp, n_fs),
        in_specs=[vmem, vmem] + [pl.BlockSpec(memory_space=pl.ANY)] * 5,
        out_specs=[vmem] * 3,
        out_shape=[
            jax.ShapeDtypeStruct((n_fs, n_tp) + tok.shape, bf16),
            jax.ShapeDtypeStruct((n_sp, depth, columns), bf16),
            jax.ShapeDtypeStruct((n_fs, shift.shape[0], width), f32),
        ],
        scratch_shapes=[dma(5), dma(2)] + [dma(n_fs)] * 4 + [dma(n_sp)] * 3 + [dma(n_fs)] * 2,
        compiler_params=pltpu.CompilerParams(collective_id=0, has_side_effects=True),
    )(tok, shift, *weights)


def map_kernel(n_sp, ma_ref, out_ref, send_sem, recv_sem):
    sp = lax.axis_index("sp")
    barrier = pltpu.get_barrier_semaphore()
    for k in range(1, n_sp):

        @pl.when(sp >= k)
        def _():
            pl.semaphore_signal(barrier, inc=1, device_id={"sp": sp - k}, device_id_type=MESH)

    @pl.when(sp < n_sp - 1)
    def _():
        pl.semaphore_wait(barrier, n_sp - 1 - sp)

    def later(k):
        return send(ma_ref, out_ref.at[sp], send_sem.at[k], recv_sem.at[sp], {"sp": sp + k})

    for k in range(1, n_sp):

        @pl.when(sp + k < n_sp)
        def _():
            later(k).start()

    for k in range(1, n_sp):

        @pl.when(sp >= k)
        def _():
            slot = out_ref.at[sp - k]
            send(slot, slot, send_sem.at[0], recv_sem.at[sp - k], {"sp": sp - k}).wait_recv()

        @pl.when(sp + k < n_sp)
        def _():
            later(k).wait_send()


def earlier_maps(n_sp, ma):
    return pl.pallas_call(
        functools.partial(map_kernel, n_sp),
        in_specs=[pl.BlockSpec(memory_space=pltpu.VMEM)],
        out_specs=pl.BlockSpec(memory_space=pltpu.VMEM),
        out_shape=jax.ShapeDtypeStruct((n_sp,) + ma.shape, bf16),
        scratch_shapes=[pltpu.SemaphoreType.DMA((n_sp,))] * 2,
        compiler_params=pltpu.CompilerParams(collective_id=2, has_side_effects=True),
    )(ma)


def reduce_partials(n_fs, part):
    dma = pltpu.SemaphoreType.DMA((n_fs,))
    block = pltpu.VMEM((n_fs,) + part.shape[2:], bf16)
    return pl.pallas_call(
        functools.partial(reduce_kernel, n_fs),
        in_specs=[pl.BlockSpec(memory_space=pltpu.VMEM)],
        out_specs=pl.BlockSpec(memory_space=pltpu.VMEM),
        out_shape=jax.ShapeDtypeStruct(part.shape[2:], bf16),
        scratch_shapes=[block, block, block, dma, dma, dma, dma],
        compiler_params=pltpu.CompilerParams(collective_id=1, has_side_effects=True),
    )(part)


def normalize_rows(norm_gain, row_piece):
    values = row_piece.astype(f32)
    scaled = values * lax.rsqrt(jnp.mean(values * values, axis=-1, keepdims=True) + norm_eps)
    return (scaled * norm_gain).astype(bf16)


def body(
    tokens, norm_gain, w_conv_gate, w_conv_in, w_conv_value, conv_taps, w_receptance, w_key,
    w_value, w_decay_down, w_decay_up, decay_base, decay_shift, w_rate_down, w_rate_up,
    rate_base, key_scale, key_mix, group_gain, w_out_conv, w_out_state,
):
    n_fs, n_sp = lax.axis_size("fs"), lax.axis_size("sp")
    fs = lax.axis_index("fs")
    width = w_key.shape[1] // n_fs

    def mine(a, axis):
        return lax.dynamic_slice_in_dim(a, fs * width, width, axis)

    n_tp = lax.axis_size("tp")
    steps = decay_shift.shape[1]
    w_conv = jnp.concatenate([mine(w_conv_gate, 1), mine(w_conv_in, 1), mine(w_conv_value, 1)], axis=1)
    w_out = jnp.concatenate([mine(w_out_conv, 0), mine(w_out_state, 0)], axis=0)
    normed, w_state, shift = gather_inputs(
        n_sp, n_fs, n_tp, normalize_rows(norm_gain, tokens[0]), decay_shift[0],
        (w_receptance, w_key, w_value, w_decay_down, w_rate_down),
    )
    normed, w_state, w_conv, w_out = lax.optimization_barrier((normed, w_state, w_conv, w_out))
    normed = normed.reshape(n_fs * steps, normed.shape[-1])
    w_state = w_state.reshape(-1, w_state.shape[-1])
    w_conv = lax.all_gather(w_conv, "sp", axis=0, tiled=True)
    w_out = lax.all_gather(w_out, "sp", axis=0)

    state_in = jnp.dot(normed, w_state, preferred_element_type=f32).astype(bf16)
    params = jnp.stack([mine(p, 0) for p in (decay_base, rate_base, key_scale, key_mix)])
    rank = w_decay_down.shape[1]
    col = lambda k: pl.BlockSpec((steps, width), lambda i, k=k: (i, k))
    low = lambda k: pl.BlockSpec((steps, rank), lambda i, k=k: (i, 3 * width // rank + k))
    full = lambda s: pl.BlockSpec(s, lambda i: (0,) * len(s))
    query, local, ma = pl.pallas_call(
        state_kernel,
        grid=(n_fs,),
        in_specs=[
            col(0), col(1), col(2), low(0), low(1), full((rank, width)), full((rank, width)),
            pl.BlockSpec((1, steps, width), lambda i: (i, 0, 0)), full((4, width)),
        ],
        out_specs=[
            col(0), col(0), pl.BlockSpec((1, 2, HEAD, width), lambda i: (i, 0, 0, 0)),
        ],
        out_shape=[
            jax.ShapeDtypeStruct((n_fs * steps, width), bf16),
            jax.ShapeDtypeStruct((n_fs * steps, width), f32),
            jax.ShapeDtypeStruct((n_fs, 2, HEAD, width), bf16),
        ],
        cost_estimate=pl.CostEstimate(flops=40_000_000_000, bytes_accessed=4_000_000, transcendentals=0),
    )(
        state_in, state_in, state_in, state_in, state_in, mine(w_decay_up, 1), mine(w_rate_up, 1),
        shift, params,
    )
    ma_all = earlier_maps(n_sp, ma)

    conv = jnp.dot(normed, w_conv, preferred_element_type=f32).astype(bf16)
    gate, source, value = (
        conv[:, i * width : (i + 1) * width].reshape(n_fs, steps, width) for i in range(3)
    )
    route = [(i, i + 1) for i in range(n_sp - 1)]
    previous = lax.ppermute(jnp.stack([source[:, -2:], value[:, -2:]]), "sp", route)
    product = jnp.concatenate([previous[0], source], axis=1).astype(f32) * jnp.concatenate(
        [previous[1], value], axis=1
    ).astype(f32)
    taps = mine(conv_taps, 1)
    filtered = taps[0] * product[:, :-2] + taps[1] * product[:, 1:-1] + taps[2] * product[:, 2:]
    conv_out = (gate.astype(f32) * filtered).astype(bf16).reshape(n_fs * steps, width)

    state_out = pl.pallas_call(
        functools.partial(finish_kernel, n_sp),
        grid=(n_fs,),
        in_specs=[
            pl.BlockSpec(memory_space=pltpu.SMEM), col(0), col(0),
            pl.BlockSpec((n_sp, 1, 2, HEAD, width), lambda i: (0, i, 0, 0, 0)), full((1, width)),
        ],
        out_specs=col(0),
        out_shape=jax.ShapeDtypeStruct((n_fs * steps, width), bf16),
    )(lax.axis_index("sp").reshape(1), query, local, ma_all, mine(group_gain, 0)[None])

    both = jnp.concatenate([conv_out, state_out], axis=1)
    w_out = jnp.swapaxes(w_out, 0, 1).reshape(both.shape[1], -1)
    partial = jnp.dot(both, w_out, preferred_element_type=f32).astype(bf16)
    mixed = reduce_partials(n_fs, partial.reshape(n_fs, n_tp, steps // n_tp, partial.shape[1]))
    return mixed[None]


def solution(mesh):
    in_specs = (
        P("fs", ("sp", "tp"), None), P(), P("sp", "tp"), P("sp", "tp"), P("sp", "tp"),
        P(None, "tp"), P("sp", "tp"), P("sp", "tp"), P("sp", "tp"), P("sp", None), P(None, "tp"),
        P("tp"), P("fs", "sp", "tp"), P("sp", None), P(None, "tp"), P("tp"), P("tp"), P("tp"),
        P("tp"), P("tp", "sp"), P("tp", "sp"),
    )
    out_specs = P("fs", ("sp", "tp"), None)
    return jax.shard_map(body, mesh=mesh, in_specs=in_specs, out_specs=out_specs, check_vma=False)
```

profile of v0, /device:TPU:25, one launch (start us, length us, event | category | flops | bytes accessed | tf_op | source)
XLA Modules:
  0.0 191.0 jit_solution(6073814934034247704)
XLA Ops:
  6.5 1.3 fusion
  7.9 1.0 constant_dynamic-slice_fusion.5
  8.9 1.0 constant_dynamic-slice_fusion.3
  9.9 0.7 pad_maximum_fusion.1
  10.6 1.7 fusion.2.tok_ref
  12.3 0.8 pad_maximum_fusion
  13.1 48.6 %shard_map.199 = (bf16[4,2,128,2048]{3,2,1,0:T(8,128)(2,1)}, bf16[4,512,640]{2,1,0:T(8,128)(2,1)}, f32[4,256,128]{2,1,0:T(8,128)}) custom-call(bf16[128,2048]{1,0:T(8,128)(2,1)} %fusion.2.tok_ref, f32[256,512]{1,0:T(8,128)} %bitcast.58, bf16[512,512]{1,0:T(8,128)(2,1)} %refs_0_.1, bf16[512,512]{1,0:T(8,128)(2,1)} %refs_1_.1, bf16[512,512]{1,0:T(8,128)(2,1)} %refs_2_.1, ...), custom_call_target="tpu_custom_call" | custom-call | tf_op jit(solution)/shard_map/pallas_call | solution.py:375
  61.7 0.7 all-gather.6.cloned.1.call-update
  62.4 0.7 constant_dynamic-slice_fusion.2
  63.1 0.8 dynamic-slice_bitcast_fusion.3
  63.9 0.8 dynamic-slice_bitcast_fusion.1
  64.7 1.4 constant_dynamic-slice_fusion
  66.1 7.6 %convolution_convert_fusion.1.recv_ref.key_ref.val_ref.dlow_ref.rlow_ref = bf16[1024,640]{1,0:T(8,128)(2,1)} fusion(bf16[1024,2048]{1,0:T(8,128)(2,1)} %bitcast.59, bf16[2048,640]{1,0:T(8,128)(2,1)} %bitcast.61), kind=kOutput, calls=%fused_computation.1 | convolution fusion | flops 2685009920 | bytes 8126464 | tf_op jit(solution)/shard_map/dot_general | solution.py:479
  73.6 0.6 pad_maximum_fusion.3.par_ref
  74.2 29.0 %shard_map.200 = (bf16[1024,128]{1,0:T(8,128)(2,1)}, f32[1024,128]{1,0:T(8,128)}, bf16[4,2,64,128]{3,2,1,0:T(8,128)(2,1)}) custom-call(bf16[1024,640]{1,0:T(8,128)(2,1)} %convolution_convert_fusion.1.recv_ref.key_ref.val_ref.dlow_ref.rlow_ref, bf16[1024,640]{1,0:T(8,128)(2,1)} %convolution_convert_fusion.1.recv_ref.key_ref.val_ref.dlow_ref.rlow_ref, ...), custom_call_target="tpu_custom_call" | custom-call | flops 40000000000 | bytes 4000000 | tf_op jit(solution)/shard_map/pallas_call | solution.py:485
  103.3 5.0 %convolution_convert_fusion.2 = bf16[1024,384]{1,0:T(8,128)(2,1)S(1)} fusion(bf16[1024,2048]{1,0:T(8,128)(2,1)} %bitcast.60, bf16[2048,384]{1,0:T(8,128)(2,1)} %all-gather.4.cloned.1.call-done), kind=kOutput, calls=%fused_computation.2 | convolution fusion | flops 1611005952 | bytes 6553600 | tf_op jit(solution)/shard_map/dot_general | solution.py:507
  108.5 1.3 collective-permute-start
  109.8 1.3 dynamic-slice_bitcast_fusion.gain_ref
  111.1 28.4 %shard_map.201.ma_ref = bf16[4,4,2,64,128]{4,3,2,1,0:T(8,128)(2,1)} custom-call(bf16[4,2,64,128]{3,2,1,0:T(8,128)(2,1)} %get-tuple-element.23.ma_ref), custom_call_target="tpu_custom_call" | custom-call | tf_op jit(solution)/shard_map/pallas_call | solution.py:424
  139.5 5.4 %shard_map.202 = bf16[1024,128]{1,0:T(8,128)(2,1)} custom-call(s32[1]{0:T(128)} %bitcast.15.place_ref, bf16[1024,128]{1,0:T(8,128)(2,1)} %get-tuple-element.21.q_ref, f32[1024,128]{1,0:T(8,128)} %get-tuple-element.22.l_ref, bf16[4,4,2,64,128]{4,3,2,1,0:T(8,128)(2,1)} %shard_map.201.ma_ref, f32[1,128]{1,0:T(1,128)} %dynamic-slice_bitcast_fusion.gain_ref), custom_call_target="tpu_custom_call" | custom-call | tf_op jit(solution)/shard_map/pallas_call | solution.py:520
  144.9 1.5 copy.22
  146.8 3.3 %convolution_convert_fusion = bf16[1024,2048]{1,0:T(8,128)(2,1)} fusion(bf16[256,2048]{0,1:T(8,128)(2,1)S(1)} %bitcast.49, bf16[1024,128]{1,0:T(8,128)(2,1)S(1)} %copy-done.2, bf16[1024,128]{1,0:T(8,128)(2,1)S(1)} %bitcast.55), kind=kOutput, calls=%fused_computation | convolution fusion | flops 1076887552 | bytes 5767168 | tf_op jit(solution)/shard_map/dot_general | solution.py:533
  150.0 32.2 %shard_map.203 = bf16[128,2048]{1,0:T(8,128)(2,1)} custom-call(bf16[4,2,128,2048]{3,2,1,0:T(8,128)(2,1)} %bitcast.48), custom_call_target="tpu_custom_call" | custom-call | tf_op jit(solution)/shard_map/pallas_call | solution.py:437
  182.2 1.9 copy.24
  (22 shorter events, 0.6 us)
Async XLA Ops:
  6.5 1.3 copy-start
  6.5 4.1 %copy-start.1 = (bf16[1,128,2048]{2,1,0:T(8,128)(2,1)S(1)}, bf16[1,128,2048]{2,1,0:T(8,128)(2,1)}, u32[]{:S(2)}) copy-start(bf16[1,128,2048]{2,1,0:T(8,128)(2,1)} %param.21) | copy-start | bytes 1572868
  6.5 96.8 %all-gather.4.cloned.1.call-start = ((), (), s32[]{:S(2)}) async-start(), calls=%async_computation | async-start | bytes 1966080 | tf_op jit(solution)/shard_map/all_gather | solution.py:476
  61.7 83.2 %all-gather.6.cloned.1.call-start = ((), (), s32[]{:S(2)}) async-start(), calls=%async_computation.1 | async-start | bytes 1310720 | tf_op jit(solution)/shard_map/all_gather | solution.py:477
  108.5 37.9 %collective-permute-start = (bf16[2,4,2,128]{3,2,1,0:T(2,128)(2,1)S(1)}, bf16[2,4,2,128]{3,2,1,0:T(2,128)(2,1)S(1)}, u32[]{:S(2)}, u32[]{:S(2)}) collective-permute-start(bf16[2,4,2,128]{3,2,1,0:T(2,128)(2,1)S(1)} %pad_maximum_fusion.2), channel_id=1, source_target_pairs={{0,8},{8,16},{16,24},{1,9},{9,17},{17,25},{2,10},{10,18},{18,26},{... | collective-permute-start | bytes 12296 | tf_op jit(solution)/shard_map/ppermute | solution.py:512
  144.9 1.9 copy-start.2
Sparse Core Ops, SparseCore 0:
  61.8 37.2 all-gather.3
  100.6 38.0 all-gather.5
where the time goes:
time: 192 us; the launch traced here: 191 us
  Pallas kernels  144 us (75%)
  matrix products  15.8 us (8%)
  between operations  13.6 us (7%)
  local copies, waits for them, and re-layouts  10.5 us (5%)
  other arithmetic  5.46 us (3%)
    pallas_call x1, Pallas kernels, gather_inputs(): pl.pallas_call(functools.partial(gather_kernel, n_sp, n_fs), in_specs=[vm...  48.6 us
    pallas_call x1, Pallas kernels, reduce_partials(): pl.pallas_call(functools.partial(reduce_kernel, n_fs), in_specs=[pl.Block...  32.2 us
    pallas_call x1, Pallas kernels, body(): pl.pallas_call(state_kernel, grid=(n_fs,), in_specs=[col(0), col(1), col(...  29 us
    pallas_call x1, Pallas kernels, earlier_maps(): pl.pallas_call(functools.partial(map_kernel, n_sp), in_specs=[pl.BlockSpe...  28.4 us
    dot_general x1, matrix products, body(): state_in = jnp.dot(normed, w_state, preferred_element_type=f32).astype(bf16)  7.57 us
    pallas_call x1, Pallas kernels, body(): pl.pallas_call(functools.partial(finish_kernel, n_sp), grid=(n_fs,), in_s...  5.38 us
    dot_general x1, matrix products, body(): conv = jnp.dot(normed, w_conv, preferred_element_type=f32).astype(bf16)  5 us
    dynamic_slice x5, local copies, waits for them, and re-layouts, mine(): return lax.dynamic_slice_in_dim(a, fs * width, width, axis)  4.11 us
  transfers between devices with their start and end apart: 3, of which 0 were waited for; matrix products, arithmetic and copies ran while one was open for 10% of the time, Pallas kernels for 33%

commit v1 on v0

v1 whole, which is shorter than its diff:
```python
import functools

import jax
import jax.numpy as jnp
from jax import lax
from jax.experimental import pallas as pl
from jax.experimental.pallas import tpu as pltpu
from jax.sharding import PartitionSpec as P

HEAD = 64
CHUNK = 64
norm_eps = 1e-06
group_eps = 0.00064
f32, bf16 = jnp.float32, jnp.bfloat16

NN = (((1,), (0,)), ((), ()))
NT = (((1,), (1,)), ((), ()))
TN = (((0,), (0,)), ((), ()))
MESH = pl.DeviceIdType.MESH


def dot1(a, b, dims):
    return lax.dot_general(a.astype(bf16), b.astype(bf16), dims, preferred_element_type=f32)


def split2(a):
    high = a.astype(bf16)
    return high, (a - high.astype(f32)).astype(bf16)


def dot3(a, b, dims):
    (ah, al), (bh, bl) = split2(a), split2(b)
    d = functools.partial(lax.dot_general, dimension_numbers=dims, preferred_element_type=f32)
    return d(ah, bh) + (d(ah, bl) + d(al, bh))


def twice(x):
    return jnp.concatenate([x, x], axis=0)


def fold(x):
    half = x.shape[0] // 2
    return x[:half] + x[half:]


def send(src, dst, send_sem, recv_sem, peer):
    return pltpu.make_async_remote_copy(
        src_ref=src, dst_ref=dst, send_sem=send_sem, recv_sem=recv_sem,
        device_id=peer, device_id_type=MESH,
    )


def head_sums(x, low):
    a = jnp.sum(jnp.where(low, x, 0.0), axis=-1, keepdims=True)
    b = jnp.sum(jnp.where(low, 0.0, x), axis=-1, keepdims=True)
    return jnp.where(low, a, b)


def sequence_maps(state_in, shift, decay_up, rate_up, par):
    tokens, width = shift.shape
    rank = decay_up.shape[0]
    decay_base, rate_base, key_scale, key_mix = par
    rounded = state_in.astype(bf16)
    recv, key, val = (rounded[:, i * width : (i + 1) * width].astype(f32) for i in range(3))
    decay_low = rounded[:, 3 * width : 3 * width + rank]
    rate_low = rounded[:, 3 * width + rank :]
    act = jnp.tanh(decay_low.astype(f32)).astype(bf16)
    pre = decay_base + lax.dot_general(act, decay_up, NN, preferred_element_type=f32)
    log_decay = shift - jnp.exp(-0.5) * jax.nn.sigmoid(pre)
    rate = jax.nn.sigmoid(
        rate_base + lax.dot_general(rate_low, rate_up, NN, preferred_element_type=f32)
    )
    low = lax.broadcasted_iota(jnp.int32, (1, width), 1) < HEAD
    scaled = key * key_scale
    erase = scaled * lax.rsqrt(head_sums(scaled * scaled, low) + norm_eps)
    write = key * (1.0 + (rate - 1.0) * key_mix)
    replace = erase * rate
    erase = -erase

    ti = lax.broadcasted_iota(jnp.int32, (tokens, tokens), 0)
    tj = lax.broadcasted_iota(jnp.int32, (tokens, tokens), 1)
    tri = jnp.where(jnp.logical_and(ti >= tj, ti // CHUNK == tj // CHUNK), 1.0, 0.0).astype(bf16)
    first = log_decay.astype(bf16)
    rest = log_decay - first.astype(f32)
    second = rest.astype(bf16)
    third = (rest - second.astype(f32)).astype(bf16)
    sums = lax.dot_general(
        tri, jnp.concatenate([first, second, third], axis=1), NN, preferred_element_type=f32
    )
    incl = sums[:, :width] + (sums[:, width : 2 * width] + sums[:, 2 * width :])
    excl = incl - log_decay

    rows = 2 * CHUNK
    ri = lax.broadcasted_iota(jnp.int32, (rows, rows), 0)
    ci = lax.broadcasted_iota(jnp.int32, (rows, rows), 1)
    same = (ri < CHUNK) == (ci < CHUNK)
    strict = jnp.logical_and(same, ri > ci)
    causal = jnp.logical_and(same, ri >= ci)
    eye = ri == ci
    st = lambda x: jnp.concatenate([jnp.where(low, x, 0.0), jnp.where(low, 0.0, x)], axis=0).astype(bf16)
    two = lambda x: twice(x.astype(bf16))

    chunks = range(tokens // CHUNK)
    sl = [slice(c * CHUNK, (c + 1) * CHUNK) for c in chunks]
    final = [incl[s.stop - 1 : s.stop] for s in sl]
    mid = [incl[s.start + CHUNK // 2 - 1 : s.start + CHUNK // 2] for s in sl]
    up = [jnp.exp(incl[s] - m) for s, m in zip(sl, mid)]
    back = [jnp.exp(m - incl[s]) for s, m in zip(sl, mid)]
    tail = [jnp.exp(f - incl[s]) for s, f in zip(sl, final)]
    left = [
        jnp.concatenate([st(erase[s] * jnp.exp(excl[s] - mid[c])), st(recv[s] * up[c])], axis=0)
        for c, s in enumerate(sl)
    ]
    right = [
        jnp.concatenate([two(replace[s] * back[c]), two(write[s] * back[c])], axis=0)
        for c, s in enumerate(sl)
    ]
    pairs = [dot1(a, b, NT) for a, b in zip(left, right)]
    v = [st(val[s]) for s in sl]
    x = [jnp.where(strict, p[:rows, :rows], 0.0) for p in pairs]
    xb = [a.astype(bf16) for a in x]
    power = [dot1(a, a, NN) for a in xb]
    ekqk = [
        jnp.concatenate(
            [
                jnp.where(strict, p[:rows, rows:], 0.0).astype(bf16),
                jnp.where(causal, p[rows:, rows:], 0.0).astype(bf16),
            ],
            axis=0,
        )
        for p in pairs
    ]
    qr = [jnp.where(causal, p[rows:, :rows], 0.0).astype(bf16) for p in pairs]
    ekv_qkv = [dot1(a, b, NN) for a, b in zip(ekqk, v)]
    inv = [jnp.where(eye, 1.0, a) for a in x]
    reached = 2
    while reached < CHUNK:
        pb = [p.astype(bf16) for p in power]
        ib = [i.astype(bf16) for i in inv]
        if reached * 2 < CHUNK:
            step = [dot1(jnp.concatenate([i, p], axis=0), p, NN) for i, p in zip(ib, pb)]
            inv = [i + s[:rows] for i, s in zip(inv, step)]
            power = [s[rows:] for s in step]
        else:
            step = [dot1(i, p, NN) for i, p in zip(ib, pb)]
            inv = [i + s for i, s in zip(inv, step)]
        reached *= 2
    e_now = [st(erase[s] * jnp.exp(excl[s])) for s in sl]
    solved = [
        dot1(i, jnp.concatenate([e, k[:rows].astype(bf16)], axis=1), NN)
        for i, e, k in zip(inv, e_now, ekv_qkv)
    ]
    seen = [dot1(a, b, NN) for a, b in zip(qr, solved)]
    query, local, step_map, carried = [], [], [], []
    for c, s in enumerate(sl):
        query.append(recv[s] * jnp.exp(incl[s]) + fold(seen[c][:, :width]))
        local.append(fold(seen[c][:, width:] + ekv_qkv[c][rows:]))
    for c, s in enumerate(sl):
        r_end, k_end = replace[s] * tail[c], (write[s] * tail[c]).astype(bf16)
        rh, rl = split2(r_end)
        sh, sl_ = split2(solved[c][:, :width])
        d = functools.partial(lax.dot_general, dimension_numbers=TN, preferred_element_type=f32)
        rh2 = twice(rh)
        moved = d(sh, rh2) + (d(sh, twice(rl)) + d(sl_, rh2))
        step_map.append(jnp.where(eye, jnp.exp(final[c]), 0.0) + jnp.where(same, moved, 0.0))
        added = d(
            jnp.concatenate([solved[c][:, width:].astype(bf16), v[c]], axis=0),
            jnp.concatenate([rh2, twice(k_end)], axis=0),
        )
        carried.append(jnp.where(same, added, 0.0))
    return query, local, step_map, carried


def layer_kernel(
    n_sp, n_fs,
    tok, gain, wr, wk, wv, wdd, wrd, wcg, wci, wcv, woc, wos, shift, wdu, wru,
    decay_base, rate_base, key_scale, key_mix, group_gain, taps,
    out_ref,
    raw, toks, ws, lows, wc, wo, shifts, acc, qm, lm, sm, cm, own_map, maps, state, both,
    halo_out, ext, part, from_pair, sums, from_fs,
    load_sem, tok_send, tok_recv, pair_send, pair_recv, low_send, low_recv, lowp_send, lowp_recv,
    shift_send, shift_recv, z_right, z_left, z_recv, map_send, map_recv, halo_sem, swap_sem,
    fs_send, fs_recv,
):
    n_tp = toks.shape[1]
    rows, dim = tok.shape
    steps, width = shifts.shape[1:]
    depth = ws.shape[1]
    rank = wdd.shape[1]
    share_rows = lows.shape[2]
    sp, fs, tp = lax.axis_index("sp"), lax.axis_index("fs"), lax.axis_index("tp")
    partner = {"tp": 1 - tp}
    if n_fs == 4:
        others = [fs + 1 - 2 * lax.rem(fs, 2), lax.rem(fs + 2, 4), 3 - fs]
    else:
        others = [lax.rem(fs + d, n_fs) for d in range(1, n_fs)]
    share = fs * n_tp + tp
    has_left, has_right = sp > 0, sp < n_sp - 1
    at_end = jnp.logical_or(sp == 0, sp == n_sp - 1)
    mine = lambda: pl.ds(pl.multiple_of(fs * width, width), width)

    def load(k, src, dst):
        return pltpu.make_async_copy(src, dst, load_sem.at[k])

    load_tok = load(0, tok, raw)
    share_of = lambda w: w.at[pl.ds(pl.multiple_of(share * share_rows, share_rows), share_rows), :]
    load_a = [
        load(1, share_of(wdd), lows.at[sp, share, :, pl.ds(0, rank)]),
        load(2, share_of(wrd), lows.at[sp, share, :, pl.ds(rank, rank)]),
    ] + [
        load(3 + i, w.at[:, mine()], ws.at[sp, :, pl.ds(i * width, width)])
        for i, w in enumerate((wr, wk, wv))
    ]
    load_b = [
        load(6 + i, w.at[:, mine()], wc.at[sp, :, pl.ds(i * width, width)])
        for i, w in enumerate((wcg, wci, wcv))
    ]
    load_c = [
        load(9 + i, w.at[mine(), :], wo.at[sp, pl.ds(i * width, width), :])
        for i, w in enumerate((woc, wos))
    ]
    load_shift = load(11, shift.at[:, mine()], shifts.at[fs])
    for copy in [load_tok] + load_a + load_b + load_c + [load_shift]:
        copy.start()

    barrier = pltpu.get_barrier_semaphore()
    peers = [partner] + [{"fs": f} for f in others]
    peers += [{"sp": lax.rem(sp + d, n_sp)} for d in range(1, n_sp)]
    for peer in peers:
        pl.semaphore_signal(barrier, inc=1, device_id=peer, device_id_type=MESH)

    load_tok.wait()
    values = raw[...].astype(f32)
    scaled = values * lax.rsqrt(jnp.mean(values * values, axis=-1, keepdims=True) + norm_eps)
    toks[fs, tp] = (scaled * gain[...]).astype(bf16)
    for copy in load_a:
        copy.wait()
    pl.semaphore_wait(barrier, len(peers))

    def z_slot(stage, j):
        if stage == 0:
            return lows.at[j, share]
        return (ws, wc, wo)[stage - 1].at[j]

    def z_copy(stage, j, to_right):
        sems = z_right if to_right else z_left
        slot = z_slot(stage, j)
        peer = {"sp": sp + 1} if to_right else {"sp": sp - 1}
        return send(slot, slot, sems.at[stage, j], z_recv.at[stage, j], peer)

    def z_start(stage):
        @pl.when(has_right)
        def _():
            z_copy(stage, sp, True).start()

        @pl.when(has_left)
        def _():
            z_copy(stage, sp, False).start()

    def z_forward(stage, k):
        @pl.when(jnp.logical_and(sp >= k, has_right))
        def _():
            z_copy(stage, sp - k, True).wait_recv()
            z_copy(stage, sp - k, True).start()

        @pl.when(jnp.logical_and(sp + k < n_sp, has_left))
        def _():
            z_copy(stage, sp + k, False).wait_recv()
            z_copy(stage, sp + k, False).start()

    def z_take(stage, j):
        @pl.when(at_end)
        def _():
            z_copy(stage, j, True).wait_recv()

    def z_drain(stage):
        for j in range(n_sp):

            @pl.when(jnp.logical_and(sp >= j, has_right))
            def _():
                z_copy(stage, j, True).wait_send()

            @pl.when(jnp.logical_and(sp <= j, has_left))
            def _():
                z_copy(stage, j, False).wait_send()

    turn = 1 - 2 * ((2 * sp) // n_sp)
    nearest = [lax.rem(sp + turn * i + n_sp, n_sp) for i in range(n_sp)]

    z_start(0)
    z_start(1)
    own_tok = toks.at[fs, tp]
    tok_out = [send(own_tok, own_tok, tok_send.at[i], tok_recv.at[fs], {"fs": f}) for i, f in enumerate(others)]
    for copy in tok_out:
        copy.start()
    pair_out = [send(own_tok, own_tok, pair_send.at[0], pair_recv.at[fs], partner)]
    pair_out[0].start()

    def forward_tokens(i):
        there = toks.at[others[i], tp]
        send(there, there, tok_send.at[i], tok_recv.at[others[i]], {"fs": others[i]}).wait_recv()
        copy = send(there, there, pair_send.at[i + 1], pair_recv.at[others[i]], partner)
        copy.start()
        pair_out.append(copy)

    for k in range(1, n_sp):
        z_forward(0, k)
    for i in range(1, n_sp):
        z_take(0, nearest[i])
    own_low = lows.at[:, share]
    low_out = [send(own_low, own_low, low_send.at[i], low_recv.at[fs], {"fs": f}) for i, f in enumerate(others)]
    lowp_out = [send(own_low, own_low, lowp_send.at[0], lowp_recv.at[fs], partner)]
    for copy in low_out + lowp_out:
        copy.start()
    z_forward(1, 1)
    for copy in load_b:
        copy.wait()
    shift_out = [
        send(
            shift.at[:, pl.ds(pl.multiple_of(f * width, width), width)], shifts.at[fs],
            shift_send.at[i], shift_recv.at[fs], {"fs": f},
        )
        for i, f in enumerate(others)
    ]
    for copy in shift_out:
        copy.start()
    for i in range(n_fs - 1):
        forward_tokens(i)
        if i + 2 < n_sp:
            z_forward(1, i + 2)
    for k in range(n_fs + 1, n_sp):
        z_forward(1, k)
    z_start(2)
    for i, f in enumerate(others):
        there = lows.at[:, f * n_tp + tp]
        send(there, there, low_send.at[i], low_recv.at[f], {"fs": f}).wait_recv()
        copy = send(there, there, lowp_send.at[i + 1], lowp_recv.at[f], partner)
        copy.start()
        lowp_out.append(copy)
    for f in [fs] + others:
        there = toks.at[f, 1 - tp]
        send(there, there, pair_send.at[0], pair_recv.at[f], partner).wait_recv()
    for f in [fs] + others:
        there = lows.at[:, f * n_tp + 1 - tp]
        send(there, there, lowp_send.at[0], lowp_recv.at[f], partner).wait_recv()

    def project(weights, column, take):
        wide = weights.shape[-1]
        if depth % 128 == 0:
            for i, j in enumerate(nearest):
                if i and take is not None:
                    z_take(take, j)
                cut = toks[:, :, :, pl.ds(pl.multiple_of(j * depth, depth), depth)]
                block = weights[j].reshape(depth, wide)
                term = lax.dot_general(
                    cut.reshape(n_fs * steps, depth), block, NN, preferred_element_type=f32
                ).reshape(n_fs, steps, wide)
                if i:
                    term = acc[:, :, pl.ds(column, wide)] + term
                acc[:, :, pl.ds(column, wide)] = term
        else:
            for i in range(1, n_sp):
                if take is not None:
                    z_take(take, nearest[i])
            whole = weights[...].reshape(dim, wide)
            acc[:, :, pl.ds(column, wide)] = lax.dot_general(
                toks[...].reshape(n_fs * steps, dim), whole, NN, preferred_element_type=f32
            ).reshape(n_fs, steps, wide)

    project(lows, 3 * width, None)
    project(ws, 0, 1)
    load_shift.wait()
    for i, f in enumerate(others):
        send(shifts.at[f], shifts.at[f], shift_send.at[i], shift_recv.at[f], {"fs": f}).wait_recv()

    par = [p[:, mine()] for p in (decay_base, rate_base, key_scale, key_mix)]
    decay_up, rate_up = wdu[:, mine()], wru[:, mine()]
    n_chunk = steps // CHUNK

    def one_sequence(f, carry):
        query, local, step_map, carried = sequence_maps(acc[f], shifts[f], decay_up, rate_up, par)
        for c in range(n_chunk):
            qm[f, pl.ds(c * CHUNK, CHUNK)] = query[c]
            lm[f, pl.ds(c * CHUNK, CHUNK)] = local[c]
            sm[f, c] = step_map[c]
            cm[f, c] = carried[c]
        k = f + 1

        @pl.when(jnp.logical_and(sp >= k, has_right))
        def _():
            z_copy(2, sp - k, True).wait_recv()
            z_copy(2, sp - k, True).start()

        @pl.when(jnp.logical_and(sp + k < n_sp, has_left))
        def _():
            z_copy(2, sp + k, False).wait_recv()
            z_copy(2, sp + k, False).start()

        return carry

    lax.fori_loop(0, n_fs, one_sequence, 0)
    for k in range(n_fs + 1, n_sp):
        z_forward(2, k)
    for copy in load_c:
        copy.wait()
    z_start(3)

    total = [jnp.concatenate([sm[f, 0], cm[f, 0]], axis=0) for f in range(n_fs)]
    square = 2 * CHUNK
    for c in range(1, n_chunk):
        cut = pl.ds(c * CHUNK, CHUNK)
        for f in range(n_fs):
            seen = dot1(qm[f, cut], total[f], NT)
            qm[f, cut] = seen[:, :square]
            lm[f, cut] = lm[f, cut] + seen[:, square:]
        total = [dot3(total[f], sm[f, c], NN) for f in range(n_fs)]
        total = [
            jnp.concatenate([t[:square], t[square:] + cm[f, c]], axis=0) for f, t in enumerate(total)
        ]
    for f in range(n_fs):
        own_map[f, 0] = fold(total[f][:square]).astype(bf16)
        own_map[f, 1] = fold(total[f][square:]).astype(bf16)

    def map_copy(k):
        return send(own_map, maps.at[sp], map_send.at[k], map_recv.at[sp], {"sp": sp + k})

    for k in range(1, n_sp):

        @pl.when(sp + k < n_sp)
        def _():
            map_copy(k).start()

    project(wc, 0, 2)
    for k in range(1, n_sp):
        z_forward(3, k)
    edge = ext.shape[1] - steps
    for f in range(n_fs):
        source = acc[f, :, pl.ds(width, width)].astype(bf16).astype(f32)
        value = acc[f, :, pl.ds(2 * width, width)].astype(bf16).astype(f32)
        product = source * value
        ext[f, pl.ds(edge, steps)] = product
        halo_out[f] = product[steps - edge :]
    halo_in = from_halo = halo_out.at[pl.ds(n_fs, n_fs)]
    halo = send(
        halo_out.at[pl.ds(0, n_fs)], halo_in, halo_sem.at[0], halo_sem.at[1], {"sp": sp + 1}
    )

    @pl.when(has_right)
    def _():
        halo.start()

    @pl.when(has_left)
    def _():
        send(from_halo, from_halo, halo_sem.at[0], halo_sem.at[1], {"sp": sp - 1}).wait_recv()
        ext[:, pl.ds(0, edge)] = halo_out[pl.ds(n_fs, n_fs)]

    @pl.when(sp == 0)
    def _():
        ext[:, pl.ds(0, edge)] = jnp.zeros((n_fs, edge, width), f32)

    tap = taps[:, mine()]
    for f in range(n_fs):
        filtered = (
            tap[0:1] * ext[f, pl.ds(edge - 2, steps)]
            + tap[1:2] * ext[f, pl.ds(edge - 1, steps)]
            + tap[2:3] * ext[f, pl.ds(edge, steps)]
        )
        gate = acc[f, :, pl.ds(0, width)].astype(bf16).astype(f32)
        both[f, :, pl.ds(0, width)] = (gate * filtered).astype(bf16)

    wi = lax.broadcasted_iota(jnp.int32, (width, width), 0)
    wj = lax.broadcasted_iota(jnp.int32, (width, width), 1)
    same = (wi < HEAD) == (wj < HEAD)
    widen = lambda x: jnp.where(same, twice(x.astype(f32)), 0.0)

    @pl.when(sp == 0)
    def _():
        state[...] = jnp.zeros(state.shape, f32)

    for hop in range(n_sp - 1):

        @pl.when(hop < sp)
        def _():
            slot = maps.at[hop]
            send(slot, slot, map_send.at[0], map_recv.at[hop], {"sp": sp - 1}).wait_recv()
            if hop == 0:
                for f in range(n_fs):
                    state[f] = widen(maps[hop, f, 1])
            else:
                new = [dot1x(state[f], widen(maps[hop, f, 0])) for f in range(n_fs)]
                for f in range(n_fs):
                    state[f] = new[f] + widen(maps[hop, f, 1])

    low = lax.broadcasted_iota(jnp.int32, (1, width), 1) < HEAD
    gains = group_gain[:, mine()]
    for f in range(n_fs):
        read = lm[f] + dot1(qm[f], state[f], NT)
        centered = read - head_sums(read, low) * (1.0 / HEAD)
        var = head_sums(centered * centered, low) * (1.0 / HEAD)
        both[f, :, pl.ds(width, width)] = (centered * lax.rsqrt(var + group_eps) * gains).astype(bf16)

    cols = wo.shape[2]
    n_blk, wide = part.shape[0], part.shape[-1]
    per = wide // cols
    if per > 1:
        for i in range(1, n_sp):
            z_take(3, nearest[i])
    blocks = nearest if per == 1 else list(range(n_blk))
    lanes = [pl.ds(pl.multiple_of(j * wide, 128), wide) for j in blocks]
    swaps, fs_out = [], []
    for i, j in enumerate(blocks):
        if per == 1:
            if i:
                z_take(3, j)
            weights = wo[j]
        else:
            weights = jnp.concatenate([wo[j * per + q] for q in range(per)], axis=1)
        term = lax.dot_general(
            both[...].reshape(n_fs * steps, both.shape[-1]), weights, NN, preferred_element_type=f32
        )
        part[i] = term.astype(bf16).reshape(n_fs, n_tp, rows, wide)
        swap = send(part.at[i, :, 1 - tp], from_pair.at[i], swap_sem.at[0, i], swap_sem.at[1, i], partner)
        swap.start()
        swaps.append(swap)
        swap.wait_recv()
        for q, f in enumerate(others + [fs]):
            total_f = part[i, f, tp].astype(f32) + from_pair[i, f].astype(f32)
            sums[i, q] = total_f.astype(bf16)
            if q < n_fs - 1:
                copy = send(sums.at[i, q], from_fs.at[i, q], fs_send.at[i, q], fs_recv.at[i, q], {"fs": f})
                copy.start()
                fs_out.append(copy)
    for i in range(n_blk):
        result = sums[i, n_fs - 1].astype(f32)
        for q in range(n_fs - 1):
            fs_out[i * (n_fs - 1) + q].wait_recv()
            result = result + from_fs[i, q].astype(f32)
        out_ref[:, lanes[i]] = result.astype(bf16)

    for copy in tok_out + pair_out + low_out + lowp_out + shift_out + swaps + fs_out:
        copy.wait_send()
    for stage in range(4):
        z_drain(stage)
    for k in range(1, n_sp):

        @pl.when(sp + k < n_sp)
        def _():
            map_copy(k).wait_send()

    @pl.when(has_right)
    def _():
        halo.wait_send()


def dot1x(a, b):
    return dot3(a, b, NN)


def body(
    tokens, norm_gain, w_conv_gate, w_conv_in, w_conv_value, conv_taps, w_receptance, w_key,
    w_value, w_decay_down, w_decay_up, decay_base, decay_shift, w_rate_down, w_rate_up,
    rate_base, key_scale, key_mix, group_gain, w_out_conv, w_out_state,
):
    n_fs, n_sp, n_tp = (lax.axis_size(a) for a in ("fs", "sp", "tp"))
    rows, dim = tokens.shape[1:]
    steps = decay_shift.shape[1]
    depth, width = w_key.shape[0], w_key.shape[1] // n_fs
    rank = w_decay_down.shape[1]
    cols = w_out_conv.shape[1]
    n_share = n_fs * n_tp
    wide = max(cols, dim // 4)
    n_blk = dim // wide
    n_chunk = steps // CHUNK
    any_, vmem = pl.BlockSpec(memory_space=pl.ANY), pl.BlockSpec(memory_space=pltpu.VMEM)
    dma = lambda *n: pltpu.SemaphoreType.DMA(n)
    row = lambda p: p.reshape(1, -1)
    edge = 8
    mixed = pl.pallas_call(
        functools.partial(layer_kernel, n_sp, n_fs),
        in_specs=[any_, vmem] + [any_] * 11 + [vmem] * 8,
        out_specs=vmem,
        out_shape=jax.ShapeDtypeStruct((rows, dim), bf16),
        scratch_shapes=[
            pltpu.VMEM((rows, dim), bf16),
            pltpu.VMEM((n_fs, n_tp, rows, dim), bf16),
            pltpu.VMEM((n_sp, depth, 3 * width), bf16),
            pltpu.VMEM((n_sp, n_share, depth // n_share, 2 * rank), bf16),
            pltpu.VMEM((n_sp, depth, 3 * width), bf16),
            pltpu.VMEM((n_sp, 2 * width, cols), bf16),
            pltpu.VMEM((n_fs, steps, width), f32),
            pltpu.VMEM((n_fs, steps, 3 * width + 2 * rank), f32),
            pltpu.VMEM((n_fs, steps, width), f32),
            pltpu.VMEM((n_fs, steps, width), f32),
            pltpu.VMEM((n_fs, n_chunk, width, width), f32),
            pltpu.VMEM((n_fs, n_chunk, width, width), f32),
            pltpu.VMEM((n_fs, 2, HEAD, width), bf16),
            pltpu.VMEM((n_sp, n_fs, 2, HEAD, width), bf16),
            pltpu.VMEM((n_fs, width, width), f32),
            pltpu.VMEM((n_fs, steps, 2 * width), bf16),
            pltpu.VMEM((2 * n_fs, edge, width), f32),
            pltpu.VMEM((n_fs, edge + steps, width), f32),
            pltpu.VMEM((n_blk, n_fs, n_tp, rows, wide), bf16),
            pltpu.VMEM((n_blk, n_fs, rows, wide), bf16),
            pltpu.VMEM((n_blk, n_fs, rows, wide), bf16),
            pltpu.VMEM((n_blk, n_fs - 1, rows, wide), bf16),
            dma(12), dma(n_fs), dma(n_fs), dma(n_fs), dma(n_fs), dma(n_fs), dma(n_fs), dma(n_fs),
            dma(n_fs), dma(n_fs), dma(n_fs), dma(4, n_sp), dma(4, n_sp), dma(4, n_sp), dma(n_sp),
            dma(n_sp), dma(2), dma(2, n_blk), dma(n_blk, n_fs), dma(n_blk, n_fs),
        ],
        compiler_params=pltpu.CompilerParams(collective_id=0, has_side_effects=True),
    )(
        tokens[0], row(norm_gain), w_receptance, w_key, w_value, w_decay_down, w_rate_down,
        w_conv_gate, w_conv_in, w_conv_value, w_out_conv, w_out_state, decay_shift[0],
        w_decay_up, w_rate_up, row(decay_base), row(rate_base), row(key_scale), row(key_mix),
        row(group_gain), conv_taps,
    )
    return mixed[None]


def solution(mesh):
    in_specs = (
        P("fs", ("sp", "tp"), None), P(), P("sp", "tp"), P("sp", "tp"), P("sp", "tp"),
        P(None, "tp"), P("sp", "tp"), P("sp", "tp"), P("sp", "tp"), P("sp", None), P(None, "tp"),
        P("tp"), P("fs", "sp", "tp"), P("sp", None), P(None, "tp"), P("tp"), P("tp"), P("tp"),
        P("tp"), P("tp", "sp"), P("tp", "sp"),
    )
    out_specs = P("fs", ("sp", "tp"), None)
    return jax.shard_map(body, mesh=mesh, in_specs=in_specs, out_specs=out_specs, check_vma=False)
```

time: 192 us -> 124 us (0.65)
  Pallas kernels: 144 us -> 121 us
  matrix products: 15.8 us -> 0 us
  between operations: 13.6 us -> 0.01 us
  local copies, waits for them, and re-layouts: 10.5 us -> 1.88 us
  other arithmetic: 5.46 us -> 0 us
    pallas_call x5 -> x1, Pallas kernels: 144 us -> 121 us  [body(): pl.pallas_call(functools.partial(layer_kernel, n_sp, n_fs), in_specs=[any...]
    dot_general x3 -> x0, matrix products: 15.8 us -> none  [the longest x1 7.57 us: body(): state_in = jnp.dot(normed, w_state, preferred_element_type=f32).astype(bf16)]
    dynamic_slice x5 -> x0, local copies, waits for them, and re-layouts: 4.11 us -> none  [mine(): return lax.dynamic_slice_in_dim(a, fs * width, width, axis)]
  transfers between devices with their start and end apart: 3 -> 0, of which waited for: 0 -> 0; matrix products, arithmetic and copies ran while one was open for 10% -> 0% of each run, Pallas kernels for 33% -> 0%
where the time goes in v1:
time: 124 us; the launch traced here: 123 us
  Pallas kernels  121 us (98%)
  local copies, waits for them, and re-layouts  1.88 us (2%)
    pallas_call x1, Pallas kernels, body(): pl.pallas_call(functools.partial(layer_kernel, n_sp, n_fs), in_specs=[any...  121 us

profile of v1, /device:TPU:25, one launch (start us, length us, event | category | flops | bytes accessed | tf_op | source)
XLA Modules:
  0.0 123.4 jit_solution(4611155335508278594)
XLA Ops:
  0.0 121.5 %shard_map.199 = bf16[128,2048]{1,0:T(8,128)(2,1)} custom-call(bf16[128,2048]{1,0:T(8,128)(2,1)} %bitcast.10, f32[1,2048]{1,0:T(1,128)} %bitcast.12, bf16[512,512]{1,0:T(8,128)(2,1)} %wr.1, bf16[512,512]{1,0:T(8,128)(2,1)} %wk.1, bf16[512,512]{1,0:T(8,128)(2,1)} %wv.1, bf16[512,128]{1,0:T(8,128)(2,1)} %wdd.1, bf16[512,128]{1,0:T(8,128)(2,1)} %wrd.1, ...), custom_call_target="tpu_custom_call" | custom-call | tf_op jit(solution)/shard_map/pallas_call | solution.py:578
  121.5 1.9 %copy.23 = bf16[1,128,2048]{2,1,0:T(8,128)(2,1)} copy(bf16[1,128,2048]{2,1,0:T(8,128)(2,1)} %bitcast.9) | data formatting | bytes 1048576

commit v2 on v1

--- a/solution.py
+++ b/solution.py
@@ -176,10 +176,10 @@
     tok, gain, wr, wk, wv, wdd, wrd, wcg, wci, wcv, woc, wos, shift, wdu, wru,
     decay_base, rate_base, key_scale, key_mix, group_gain, taps,
     out_ref,
-    raw, toks, ws, lows, wc, wo, shifts, acc, qm, lm, sm, cm, own_map, maps, state, both,
-    halo_out, ext, part, from_pair, sums, from_fs,
-    load_sem, tok_send, tok_recv, pair_send, pair_recv, low_send, low_recv, lowp_send, lowp_recv,
-    shift_send, shift_recv, z_right, z_left, z_recv, map_send, map_recv, halo_sem, swap_sem,
+    raw, toks, ws, lows, wc, wo, shifts, acc, qm, lm, sm, cm, tm, state_out, state_in, state, both,
+    halo_buf, ext, part, from_pair, sums, from_x, from_y, relay, relayed,
+    load_sem, tok_sem, tok_recv, pair_send, pair_recv, low_send, low_recv, lowp_send, lowp_recv,
+    shift_send, shift_recv, z_right, z_left, z_recv, state_sem, halo_sem, swap_sem,
     fs_send, fs_recv,
 ):
     n_tp = toks.shape[1]
@@ -225,86 +225,159 @@
 
     barrier = pltpu.get_barrier_semaphore()
     peers = [partner] + [{"fs": f} for f in others]
-    peers += [{"sp": lax.rem(sp + d, n_sp)} for d in range(1, n_sp)]
     for peer in peers:
         pl.semaphore_signal(barrier, inc=1, device_id=peer, device_id_type=MESH)
+
+    @pl.when(has_left)
+    def _():
+        pl.semaphore_signal(barrier, inc=1, device_id={"sp": sp - 1}, device_id_type=MESH)
+
+    @pl.when(has_right)
+    def _():
+        pl.semaphore_signal(barrier, inc=1, device_id={"sp": sp + 1}, device_id_type=MESH)
 
     load_tok.wait()
     values = raw[...].astype(f32)
     scaled = values * lax.rsqrt(jnp.mean(values * values, axis=-1, keepdims=True) + norm_eps)
     toks[fs, tp] = (scaled * gain[...]).astype(bf16)
-    for copy in load_a:
+    for copy in load_a + load_b + load_c:
         copy.wait()
-    pl.semaphore_wait(barrier, len(peers))
-
-    def z_slot(stage, j):
+    pl.semaphore_wait(barrier, len(peers) + has_left.astype(jnp.int32) + has_right.astype(jnp.int32))
+
+    cols = wo.shape[2]
+    n_blk, wide = part.shape[0], part.shape[-1]
+    row_pieces = max(1, depth // 128)
+    n_piece = (1, row_pieces, row_pieces, max(1, cols // wide))
+
+    def z_slot(stage, j, q):
         if stage == 0:
             return lows.at[j, share]
-        return (ws, wc, wo)[stage - 1].at[j]
-
-    def z_copy(stage, j, to_right):
+        if stage < 3:
+            size = depth // row_pieces
+            return (ws, wc)[stage - 1].at[j, pl.ds(q * size, size)]
+        return wo.at[j, :, pl.ds(q * wide, wide)] if n_piece[3] > 1 else wo.at[j]
+
+    def z_copy(stage, j, q, to_right):
         sems = z_right if to_right else z_left
-        slot = z_slot(stage, j)
+        slot = z_slot(stage, j, q)
         peer = {"sp": sp + 1} if to_right else {"sp": sp - 1}
-        return send(slot, slot, sems.at[stage, j], z_recv.at[stage, j], peer)
-
-    def z_start(stage):
-        @pl.when(has_right)
+        return send(slot, slot, sems.at[stage, j, q], z_recv.at[stage, j, q], peer)
+
+    def z_own(stage, to_right, when, pieces=None):
+        @pl.when(jnp.logical_and(when, has_right if to_right else has_left))
         def _():
-            z_copy(stage, sp, True).start()
-
-        @pl.when(has_left)
-        def _():
-            z_copy(stage, sp, False).start()
-
-    def z_forward(stage, k):
-        @pl.when(jnp.logical_and(sp >= k, has_right))
-        def _():
-            z_copy(stage, sp - k, True).wait_recv()
-            z_copy(stage, sp - k, True).start()
-
-        @pl.when(jnp.logical_and(sp + k < n_sp, has_left))
-        def _():
-            z_copy(stage, sp + k, False).wait_recv()
-            z_copy(stage, sp + k, False).start()
-
-    def z_take(stage, j):
+            for q in range(n_piece[stage]) if pieces is None else pieces:
+                z_copy(stage, sp, q, to_right).start()
+
+    def z_hop(stage, k, to_right, when=True, pieces=None, wait=True, start=True):
+        ahead = sp if to_right else n_sp - 1 - sp
+        here = jnp.logical_and(when, has_right if to_right else has_left)
+        j = sp - k if to_right else sp + k
+        pieces = range(n_piece[stage]) if pieces is None else pieces
+
+        if k:
+
+            @pl.when(jnp.logical_and(here, ahead >= k))
+            def _():
+                for q in pieces:
+                    if wait:
+                        z_copy(stage, j, q, to_right).wait_recv()
+                    if start:
+                        z_copy(stage, j, q, to_right).start()
+
+        if start and n_piece[stage] - 1 in pieces and 0 < stage < 3:
+            z_own(stage + 1, to_right, jnp.logical_and(when, ahead == k))
+
+    def z_both(stage, k, pieces=None, **how):
+        z_hop(stage, k, True, True, pieces, **how)
+        z_hop(stage, k, False, True, pieces, **how)
+
+    right_short = 2 * sp < n_sp
+
+    def z_short(stage, k):
+        z_hop(stage, k, True, right_short)
+        z_hop(stage, k, False, jnp.logical_not(right_short))
+
+    def z_long(stage, k):
+        z_hop(stage, k, True, jnp.logical_not(right_short))
+        z_hop(stage, k, False, right_short)
+
+    def z_take(stage, j, pieces=None):
         @pl.when(at_end)
         def _():
-            z_copy(stage, j, True).wait_recv()
+            for q in range(n_piece[stage]) if pieces is None else pieces:
+                z_copy(stage, j, q, True).wait_recv()
 
     def z_drain(stage):
         for j in range(n_sp):
 
             @pl.when(jnp.logical_and(sp >= j, has_right))
             def _():
-                z_copy(stage, j, True).wait_send()
+                for q in range(n_piece[stage]):
+                    z_copy(stage, j, q, True).wait_send()
 
             @pl.when(jnp.logical_and(sp <= j, has_left))
             def _():
-                z_copy(stage, j, False).wait_send()
+                for q in range(n_piece[stage]):
+                    z_copy(stage, j, q, False).wait_send()
 
     turn = 1 - 2 * ((2 * sp) // n_sp)
     nearest = [lax.rem(sp + turn * i + n_sp, n_sp) for i in range(n_sp)]
 
-    z_start(0)
-    z_start(1)
-    own_tok = toks.at[fs, tp]
-    tok_out = [send(own_tok, own_tok, tok_send.at[i], tok_recv.at[fs], {"fs": f}) for i, f in enumerate(others)]
-    for copy in tok_out:
+    last = row_pieces - 1
+    batch = [range(0, (last + 1) // 2), range((last + 1) // 2, last + 1)]
+
+    def own_state(pieces):
+        z_own(1, True, True, pieces)
+        z_own(1, False, True, pieces)
+
+    z_own(0, True, True)
+    z_own(0, False, True)
+    own_state(range(0, last // 2))
+
+    half = rows // 2
+    tok_slot = lambda f, t, h: toks.at[f, t, pl.ds(h * half, half)]
+    tok_out, pair_out = [], []
+
+    def tok_send_to(f, h, peer, sem):
+        slot = tok_slot(f, tp, h)
+        copy = send(slot, slot, tok_sem.at[sem], tok_recv.at[f, h], {"fs": peer})
         copy.start()
-    pair_out = [send(own_tok, own_tok, pair_send.at[0], pair_recv.at[fs], partner)]
-    pair_out[0].start()
-
-    def forward_tokens(i):
-        there = toks.at[others[i], tp]
-        send(there, there, tok_send.at[i], tok_recv.at[others[i]], {"fs": others[i]}).wait_recv()
-        copy = send(there, there, pair_send.at[i + 1], pair_recv.at[others[i]], partner)
+        tok_out.append(copy)
+
+    def tok_wait(f, h):
+        slot = tok_slot(f, tp, h)
+        send(slot, slot, tok_sem.at[0], tok_recv.at[f, h], {"fs": f}).wait_recv()
+
+    def tok_pair(f, h, sem):
+        slot = tok_slot(f, tp, h)
+        copy = send(slot, slot, pair_send.at[sem], pair_recv.at[f, h], partner)
         copy.start()
         pair_out.append(copy)
 
-    for k in range(1, n_sp):
-        z_forward(0, k)
+    near_x, near_y, far = others
+    tok_send_to(fs, 0, near_x, 0)
+    tok_send_to(fs, 1, near_y, 1)
+    tok_send_to(fs, 1, near_x, 2)
+    tok_send_to(fs, 0, near_y, 3)
+    tok_pair(fs, 0, 0)
+    tok_pair(fs, 1, 1)
+
+    z_both(0, 1)
+    own_state(range(last // 2, last))
+    for k in range(2, n_sp):
+        z_both(0, k)
+    own_state(range(last, last + 1))
+    for stage in (1, 2):
+        z_hop(stage, 0, True)
+        z_hop(stage, 0, False)
+    z_both(1, 1, batch[0])
+    tok_wait(near_x, 0)
+    tok_send_to(near_x, 0, near_y, 4)
+    tok_wait(near_y, 1)
+    tok_send_to(near_y, 1, near_x, 5)
+    tok_pair(near_x, 0, 2)
+    tok_pair(near_y, 1, 3)
     for i in range(1, n_sp):
         z_take(0, nearest[i])
     own_low = lows.at[:, share]
@@ -312,9 +385,6 @@
     lowp_out = [send(own_low, own_low, lowp_send.at[0], lowp_recv.at[fs], partner)]
     for copy in low_out + lowp_out:
         copy.start()
-    z_forward(1, 1)
-    for copy in load_b:
-        copy.wait()
     shift_out = [
         send(
             shift.at[:, pl.ds(pl.multiple_of(f * width, width), width)], shifts.at[fs],
@@ -324,30 +394,41 @@
     ]
     for copy in shift_out:
         copy.start()
-    for i in range(n_fs - 1):
-        forward_tokens(i)
-        if i + 2 < n_sp:
-            z_forward(1, i + 2)
-    for k in range(n_fs + 1, n_sp):
-        z_forward(1, k)
-    z_start(2)
-    for i, f in enumerate(others):
-        there = lows.at[:, f * n_tp + tp]
-        send(there, there, low_send.at[i], low_recv.at[f], {"fs": f}).wait_recv()
-        copy = send(there, there, lowp_send.at[i + 1], lowp_recv.at[f], partner)
-        copy.start()
-        lowp_out.append(copy)
+    z_both(1, 1, batch[1])
+    tok_wait(near_x, 1)
+    tok_pair(near_x, 1, 4)
+    tok_wait(near_y, 0)
+    tok_pair(near_y, 0, 5)
+    z_both(1, 2, batch[0])
+    tok_wait(far, 0)
+    tok_pair(far, 0, 6)
+    tok_wait(far, 1)
+    tok_pair(far, 1, 7)
+    z_both(1, 2, batch[1])
+    for k in range(3, n_sp):
+        z_both(1, k)
+    z_short(2, 1)
     for f in [fs] + others:
-        there = toks.at[f, 1 - tp]
-        send(there, there, pair_send.at[0], pair_recv.at[f], partner).wait_recv()
-    for f in [fs] + others:
-        there = lows.at[:, f * n_tp + 1 - tp]
-        send(there, there, lowp_send.at[0], lowp_recv.at[f], partner).wait_recv()
-
-    def project(weights, column, take):
+        for h in range(2):
+            slot = tok_slot(f, 1 - tp, h)
+            send(slot, slot, pair_send.at[0], pair_recv.at[f, h], partner).wait_recv()
+
+    def take_low():
+        for i, f in enumerate(others):
+            there = lows.at[:, f * n_tp + tp]
+            send(there, there, low_send.at[i], low_recv.at[f], {"fs": f}).wait_recv()
+            copy = send(there, there, lowp_send.at[i + 1], lowp_recv.at[f], partner)
+            copy.start()
+            lowp_out.append(copy)
+        for f in [fs] + others:
+            there = lows.at[:, f * n_tp + 1 - tp]
+            send(there, there, lowp_send.at[0], lowp_recv.at[f], partner).wait_recv()
+
+    def project(weights, column, take, order):
         wide = weights.shape[-1]
         if depth % 128 == 0:
-            for i, j in enumerate(nearest):
+            for i in order:
+                j = nearest[i]
                 if i and take is not None:
                     z_take(take, j)
                 cut = toks[:, :, :, pl.ds(pl.multiple_of(j * depth, depth), depth)]
@@ -358,7 +439,7 @@
                 if i:
                     term = acc[:, :, pl.ds(column, wide)] + term
                 acc[:, :, pl.ds(column, wide)] = term
-        else:
+        elif n_sp - 1 in order:
             for i in range(1, n_sp):
                 if take is not None:
                     z_take(take, nearest[i])
@@ -367,8 +448,10 @@
                 toks[...].reshape(n_fs * steps, dim), whole, NN, preferred_element_type=f32
             ).reshape(n_fs, steps, wide)
 
-    project(lows, 3 * width, None)
-    project(ws, 0, 1)
+    project(ws, 0, 1, range(n_sp - 1))
+    take_low()
+    project(lows, 3 * width, None, range(n_sp))
+    project(ws, 0, 1, [n_sp - 1])
     load_shift.wait()
     for i, f in enumerate(others):
         send(shifts.at[f], shifts.at[f], shift_send.at[i], shift_recv.at[f], {"fs": f}).wait_recv()
@@ -384,26 +467,14 @@
             lm[f, pl.ds(c * CHUNK, CHUNK)] = local[c]
             sm[f, c] = step_map[c]
             cm[f, c] = carried[c]
-        k = f + 1
-
-        @pl.when(jnp.logical_and(sp >= k, has_right))
+
+        @pl.when(f == n_fs // 2 - 1)
         def _():
-            z_copy(2, sp - k, True).wait_recv()
-            z_copy(2, sp - k, True).start()
-
-        @pl.when(jnp.logical_and(sp + k < n_sp, has_left))
-        def _():
-            z_copy(2, sp + k, False).wait_recv()
-            z_copy(2, sp + k, False).start()
+            z_long(2, 1)
 
         return carry
 
     lax.fori_loop(0, n_fs, one_sequence, 0)
-    for k in range(n_fs + 1, n_sp):
-        z_forward(2, k)
-    for copy in load_c:
-        copy.wait()
-    z_start(3)
 
     total = [jnp.concatenate([sm[f, 0], cm[f, 0]], axis=0) for f in range(n_fs)]
     square = 2 * CHUNK
@@ -418,41 +489,89 @@
             jnp.concatenate([t[:square], t[square:] + cm[f, c]], axis=0) for f, t in enumerate(total)
         ]
     for f in range(n_fs):
-        own_map[f, 0] = fold(total[f][:square]).astype(bf16)
-        own_map[f, 1] = fold(total[f][square:]).astype(bf16)
-
-    def map_copy(k):
-        return send(own_map, maps.at[sp], map_send.at[k], map_recv.at[sp], {"sp": sp + k})
-
-    for k in range(1, n_sp):
-
-        @pl.when(sp + k < n_sp)
+        tm[f] = total[f]
+    state_copy = send(state_out, state_in, state_sem.at[0], state_sem.at[1], {"sp": sp + 1})
+
+    @pl.when(sp == 0)
+    def _():
+        state[...] = jnp.zeros(state.shape, f32)
+        for f in range(n_fs):
+            state_out[f] = fold(tm[f, pl.ds(square, square)]).astype(bf16)
+
+        @pl.when(has_right)
         def _():
-            map_copy(k).start()
-
-    project(wc, 0, 2)
-    for k in range(1, n_sp):
-        z_forward(3, k)
+            state_copy.start()
+
     edge = ext.shape[1] - steps
+    halo = send(
+        halo_buf.at[0], halo_buf.at[1], halo_sem.at[0], halo_sem.at[1], {"sp": sp + 1}
+    )
+
+    def convolve():
+        project(wc, 0, 2, range(n_sp))
+        for f in range(n_fs):
+            source = acc[f, :, pl.ds(width, width)].astype(bf16).astype(f32)
+            value = acc[f, :, pl.ds(2 * width, width)].astype(bf16).astype(f32)
+            product = source * value
+            ext[f, pl.ds(edge, steps)] = product
+            halo_buf[0, f] = product[steps - edge :]
+
+        @pl.when(has_right)
+        def _():
+            halo.start()
+
+    farthest = n_sp - 2
+    for k in range(2, farthest):
+        z_both(2, k)
+    if farthest > 1:
+        z_both(2, farthest, start=False)
+
+    @pl.when(jnp.logical_not(at_end))
+    def _():
+        convolve()
+
+    if farthest > 1:
+        z_both(2, farthest, batch[0], wait=False)
+    wi = lax.broadcasted_iota(jnp.int32, (width, width), 0)
+    wj = lax.broadcasted_iota(jnp.int32, (width, width), 1)
+    same = (wi < HEAD) == (wj < HEAD)
+
+    @pl.when(has_left)
+    def _():
+        state_copy.wait_recv()
+        for f in range(n_fs):
+            state[f] = jnp.where(same, twice(state_in[f].astype(f32)), 0.0)
+
+    @pl.when(jnp.logical_and(has_left, has_right))
+    def _():
+        new = [dot3(state[f], tm[f, pl.ds(0, square)], NN) for f in range(n_fs)]
+        for f in range(n_fs):
+            state_out[f] = fold(new[f] + tm[f, pl.ds(square, square)]).astype(bf16)
+        state_copy.start()
+
+    if farthest > 1:
+        z_both(2, farthest, batch[1], wait=False)
+    z_short(3, 1)
+    low = lax.broadcasted_iota(jnp.int32, (1, width), 1) < HEAD
+    gains = group_gain[:, mine()]
     for f in range(n_fs):
-        source = acc[f, :, pl.ds(width, width)].astype(bf16).astype(f32)
-        value = acc[f, :, pl.ds(2 * width, width)].astype(bf16).astype(f32)
-        product = source * value
-        ext[f, pl.ds(edge, steps)] = product
-        halo_out[f] = product[steps - edge :]
-    halo_in = from_halo = halo_out.at[pl.ds(n_fs, n_fs)]
-    halo = send(
-        halo_out.at[pl.ds(0, n_fs)], halo_in, halo_sem.at[0], halo_sem.at[1], {"sp": sp + 1}
-    )
-
-    @pl.when(has_right)
-    def _():
-        halo.start()
+        read = lm[f] + dot1(qm[f], state[f], NT)
+        centered = read - head_sums(read, low) * (1.0 / HEAD)
+        var = head_sums(centered * centered, low) * (1.0 / HEAD)
+        both[f, :, pl.ds(width, width)] = (centered * lax.rsqrt(var + group_eps) * gains).astype(bf16)
+
+    @pl.when(at_end)
+    def _():
+        convolve()
+
+    z_long(3, 1)
+    for k in range(2, n_sp):
+        z_both(3, k)
 
     @pl.when(has_left)
     def _():
-        send(from_halo, from_halo, halo_sem.at[0], halo_sem.at[1], {"sp": sp - 1}).wait_recv()
-        ext[:, pl.ds(0, edge)] = halo_out[pl.ds(n_fs, n_fs)]
+        halo.wait_recv()
+        ext[:, pl.ds(0, edge)] = halo_buf[1]
 
     @pl.when(sp == 0)
     def _():
@@ -468,53 +587,57 @@
         gate = acc[f, :, pl.ds(0, width)].astype(bf16).astype(f32)
         both[f, :, pl.ds(0, width)] = (gate * filtered).astype(bf16)
 
-    wi = lax.broadcasted_iota(jnp.int32, (width, width), 0)
-    wj = lax.broadcasted_iota(jnp.int32, (width, width), 1)
-    same = (wi < HEAD) == (wj < HEAD)
-    widen = lambda x: jnp.where(same, twice(x.astype(f32)), 0.0)
-
-    @pl.when(sp == 0)
-    def _():
-        state[...] = jnp.zeros(state.shape, f32)
-
-    for hop in range(n_sp - 1):
-
-        @pl.when(hop < sp)
-        def _():
-            slot = maps.at[hop]
-            send(slot, slot, map_send.at[0], map_recv.at[hop], {"sp": sp - 1}).wait_recv()
-            if hop == 0:
-                for f in range(n_fs):
-                    state[f] = widen(maps[hop, f, 1])
-            else:
-                new = [dot1x(state[f], widen(maps[hop, f, 0])) for f in range(n_fs)]
-                for f in range(n_fs):
-                    state[f] = new[f] + widen(maps[hop, f, 1])
-
-    low = lax.broadcasted_iota(jnp.int32, (1, width), 1) < HEAD
-    gains = group_gain[:, mine()]
-    for f in range(n_fs):
-        read = lm[f] + dot1(qm[f], state[f], NT)
-        centered = read - head_sums(read, low) * (1.0 / HEAD)
-        var = head_sums(centered * centered, low) * (1.0 / HEAD)
-        both[f, :, pl.ds(width, width)] = (centered * lax.rsqrt(var + group_eps) * gains).astype(bf16)
-
-    cols = wo.shape[2]
-    n_blk, wide = part.shape[0], part.shape[-1]
-    per = wide // cols
-    if per > 1:
+    per, n_cut, lag = max(1, wide // cols), n_piece[3], 2
+    if n_cut == 1:
         for i in range(1, n_sp):
             z_take(3, nearest[i])
-    blocks = nearest if per == 1 else list(range(n_blk))
-    lanes = [pl.ds(pl.multiple_of(j * wide, 128), wide) for j in blocks]
-    swaps, fs_out = [], []
-    for i, j in enumerate(blocks):
+    upper, lower = pl.ds(0, half), pl.ds(half, half)
+    order = [near_x, far, near_y, fs]
+    swaps, first_out, second_out, lanes = [], [], [], []
+
+    def first_step(i):
+        over_x = send(
+            sums.at[i, pl.ds(0, 2), upper], from_x.at[i], fs_send.at[i, 0], fs_recv.at[i, 0],
+            {"fs": near_x},
+        )
+        over_y = send(
+            sums.at[i, pl.ds(1, 2), lower], from_y.at[i], fs_send.at[i, 1], fs_recv.at[i, 1],
+            {"fs": near_y},
+        )
+        over_x.start()
+        over_y.start()
+        first_out.append((over_x, over_y))
+
+    def second_step(i):
+        over_x, over_y = first_out[i]
+        over_x.wait_recv()
+        relay[i, 0] = (sums[i, 2, upper].astype(f32) + from_x[i, 1].astype(f32)).astype(bf16)
+        to_y = send(relay.at[i, 0], relayed.at[i, 0], fs_send.at[i, 2], fs_recv.at[i, 2], {"fs": near_y})
+        to_y.start()
+        over_y.wait_recv()
+        relay[i, 1] = (sums[i, 0, lower].astype(f32) + from_y[i, 0].astype(f32)).astype(bf16)
+        to_x = send(relay.at[i, 1], relayed.at[i, 1], fs_send.at[i, 3], fs_recv.at[i, 3], {"fs": near_x})
+        to_x.start()
+        second_out.append((to_y, to_x))
+
+    def finish_block(i):
+        to_y, to_x = second_out[i]
+        to_y.wait_recv()
+        to_x.wait_recv()
+        for cut_rows, h, got in ((upper, 0, from_x[i, 0]), (lower, 1, from_y[i, 1])):
+            result = sums[i, 3, cut_rows].astype(f32) + got.astype(f32) + relayed[i, h].astype(f32)
+            out_ref[cut_rows, lanes[i]] = result.astype(bf16)
+
+    for i in range(n_blk):
         if per == 1:
-            if i:
-                z_take(3, j)
-            weights = wo[j]
+            j, q = nearest[i // n_cut], i % n_cut
+            if i >= n_cut and n_cut > 1:
+                z_take(3, j, [q])
+            weights = wo[j, :, pl.ds(q * wide, wide)]
+            lanes.append(pl.ds(pl.multiple_of(j * cols + q * wide, 128), wide))
         else:
-            weights = jnp.concatenate([wo[j * per + q] for q in range(per)], axis=1)
+            weights = jnp.concatenate([wo[i * per + q] for q in range(per)], axis=1)
+            lanes.append(pl.ds(i * wide, wide))
         term = lax.dot_general(
             both[...].reshape(n_fs * steps, both.shape[-1]), weights, NN, preferred_element_type=f32
         )
@@ -522,38 +645,31 @@
         swap = send(part.at[i, :, 1 - tp], from_pair.at[i], swap_sem.at[0, i], swap_sem.at[1, i], partner)
         swap.start()
         swaps.append(swap)
+        if i >= lag:
+            second_step(i - lag)
         swap.wait_recv()
-        for q, f in enumerate(others + [fs]):
-            total_f = part[i, f, tp].astype(f32) + from_pair[i, f].astype(f32)
-            sums[i, q] = total_f.astype(bf16)
-            if q < n_fs - 1:
-                copy = send(sums.at[i, q], from_fs.at[i, q], fs_send.at[i, q], fs_recv.at[i, q], {"fs": f})
-                copy.start()
-                fs_out.append(copy)
-    for i in range(n_blk):
-        result = sums[i, n_fs - 1].astype(f32)
-        for q in range(n_fs - 1):
-            fs_out[i * (n_fs - 1) + q].wait_recv()
-            result = result + from_fs[i, q].astype(f32)
-        out_ref[:, lanes[i]] = result.astype(bf16)
-
-    for copy in tok_out + pair_out + low_out + lowp_out + shift_out + swaps + fs_out:
+        for q, f in enumerate(order):
+            sums[i, q] = (part[i, f, tp].astype(f32) + from_pair[i, f].astype(f32)).astype(bf16)
+        first_step(i)
+        if i >= 2 * lag:
+            finish_block(i - 2 * lag)
+    for i in range(max(0, n_blk - lag), n_blk):
+        second_step(i)
+    for i in range(max(0, n_blk - 2 * lag), n_blk):
+        finish_block(i)
+
+    for copy in tok_out + pair_out + low_out + lowp_out + shift_out + swaps:
         copy.wait_send()
+    for pair in first_out + second_out:
+        for copy in pair:
+            copy.wait_send()
     for stage in range(4):
         z_drain(stage)
-    for k in range(1, n_sp):
-
-        @pl.when(sp + k < n_sp)
-        def _():
-            map_copy(k).wait_send()
 
     @pl.when(has_right)
     def _():
+        state_copy.wait_send()
         halo.wait_send()
-
-
-def dot1x(a, b):
-    return dot3(a, b, NN)
 
 
 def body(
@@ -568,9 +684,10 @@
     rank = w_decay_down.shape[1]
     cols = w_out_conv.shape[1]
     n_share = n_fs * n_tp
-    wide = max(cols, dim // 4)
+    wide = dim // 8
     n_blk = dim // wide
     n_chunk = steps // CHUNK
+    n_piece = max(1, depth // 128)
     any_, vmem = pl.BlockSpec(memory_space=pl.ANY), pl.BlockSpec(memory_space=pltpu.VMEM)
     dma = lambda *n: pltpu.SemaphoreType.DMA(n)
     row = lambda p: p.reshape(1, -1)
@@ -593,19 +710,24 @@
             pltpu.VMEM((n_fs, steps, width), f32),
             pltpu.VMEM((n_fs, n_chunk, width, width), f32),
             pltpu.VMEM((n_fs, n_chunk, width, width), f32),
-            pltpu.VMEM((n_fs, 2, HEAD, width), bf16),
-            pltpu.VMEM((n_sp, n_fs, 2, HEAD, width), bf16),
+            pltpu.VMEM((n_fs, 2 * width, width), f32),
+            pltpu.VMEM((n_fs, HEAD, width), bf16),
+            pltpu.VMEM((n_fs, HEAD, width), bf16),
             pltpu.VMEM((n_fs, width, width), f32),
             pltpu.VMEM((n_fs, steps, 2 * width), bf16),
-            pltpu.VMEM((2 * n_fs, edge, width), f32),
+            pltpu.VMEM((2, n_fs, edge, width), f32),
             pltpu.VMEM((n_fs, edge + steps, width), f32),
             pltpu.VMEM((n_blk, n_fs, n_tp, rows, wide), bf16),
             pltpu.VMEM((n_blk, n_fs, rows, wide), bf16),
             pltpu.VMEM((n_blk, n_fs, rows, wide), bf16),
-            pltpu.VMEM((n_blk, n_fs - 1, rows, wide), bf16),
-            dma(12), dma(n_fs), dma(n_fs), dma(n_fs), dma(n_fs), dma(n_fs), dma(n_fs), dma(n_fs),
-            dma(n_fs), dma(n_fs), dma(n_fs), dma(4, n_sp), dma(4, n_sp), dma(4, n_sp), dma(n_sp),
-            dma(n_sp), dma(2), dma(2, n_blk), dma(n_blk, n_fs), dma(n_blk, n_fs),
+            pltpu.VMEM((n_blk, 2, rows // 2, wide), bf16),
+            pltpu.VMEM((n_blk, 2, rows // 2, wide), bf16),
+            pltpu.VMEM((n_blk, 2, rows // 2, wide), bf16),
+            pltpu.VMEM((n_blk, 2, rows // 2, wide), bf16),
+            dma(12), dma(6), dma(n_fs, 2), dma(2 * n_fs), dma(n_fs, 2), dma(n_fs), dma(n_fs), dma(n_fs),
+            dma(n_fs), dma(n_fs), dma(n_fs), dma(4, n_sp, n_piece), dma(4, n_sp, n_piece),
+            dma(4, n_sp, n_piece), dma(2),
+            dma(2), dma(2, n_blk), dma(n_blk, 4), dma(n_blk, 4),
         ],
         compiler_params=pltpu.CompilerParams(collective_id=0, has_side_effects=True),
     )(

time: 124 us -> 91.7 us (0.74)
  the two profiles are of different devices: /device:TPU:25 before, /device:TPU:0 now
where the time goes in v2:
time: 91.7 us; the launch traced here: 91.5 us
  Pallas kernels  89.6 us (98%)
  local copies, waits for them, and re-layouts  1.88 us (2%)
    pallas_call x1, Pallas kernels, body(): pl.pallas_call(functools.partial(layer_kernel, n_sp, n_fs), in_specs=[any...  89.6 us
    unnamed x1, local copies, waits for them, and re-layouts  1.88 us

profile of v2, /device:TPU:0, one launch (start us, length us, event | category | flops | bytes accessed | tf_op | source)
XLA Modules:
  0.0 91.5 jit_solution(6988834977973625842)
XLA Ops:
  0.0 89.6 %shard_map.199 = bf16[128,2048]{1,0:T(8,128)(2,1)} custom-call(bf16[128,2048]{1,0:T(8,128)(2,1)} %bitcast.10, f32[1,2048]{1,0:T(1,128)} %bitcast.12, bf16[512,512]{1,0:T(8,128)(2,1)} %wr.1, bf16[512,512]{1,0:T(8,128)(2,1)} %wk.1, bf16[512,512]{1,0:T(8,128)(2,1)} %wv.1, bf16[512,128]{1,0:T(8,128)(2,1)} %wdd.1, bf16[512,128]{1,0:T(8,128)(2,1)} %wrd.1, ...), custom_call_target="tpu_custom_call" | custom-call | tf_op jit(solution)/shard_map/pallas_call | solution.py:695
  89.7 1.9 %copy.23 = bf16[1,128,2048]{2,1,0:T(8,128)(2,1)} copy(bf16[1,128,2048]{2,1,0:T(8,128)(2,1)} %bitcast.9) | data formatting | bytes 1048576
